TPU v7x, 32 devices: a whole 2x2x4 slice. The times are simulated.
32 devices in a mesh: sp: 8 (over z, x), tp: 4 (over y, core).
Axes of the slice: x: 2, y: 2, z: 4, core: 2. Of those that a mesh axis runs over, the one named last changes fastest.
Arguments:
- layer_input: bfloat16 [8, 4096, 2048], P(None, ('sp', 'tp')), may hold values from -6 to 6
- norm_gain: bfloat16 [2048], replicated, may hold values from 0.099609375 to 1.8984375
- key_weight: bfloat16 [2048, 1024], replicated, may hold values from -0.125 to 0.125
- value_weight: bfloat16 [2048, 1024], replicated, may hold values from -0.125 to 0.125
- new_query: bfloat16 [8, 1024], P('sp', 'tp'), may hold values from -12 to 12
- score_offset: float32 [8], replicated, may hold values from -10 to -3.5
Outputs:
- key_cache: bfloat16 [8, 4096, 1024], P('sp', None, 'tp')
- value_cache: bfloat16 [8, 4096, 1024], P('sp', None, 'tp')
- first_read: float32 [8, 1024], P('sp', 'tp')
All inputs are finite; a program needn't handle non-finite values.
Results may differ from a plain program's by a relative error of at most 0.0082.
Values may be sent and summed in bfloat16 or wider, within the bound.
A program may use at most 128 MiB of HBM per device.

v0:
```python
import functools

import jax
import jax.numpy as jnp
from jax import lax
from jax.experimental import pallas as pl
from jax.experimental.pallas import tpu as pltpu
from jax.sharding import PartitionSpec as P

norm_epsilon = 1e-06
MESH = pl.DeviceIdType.MESH
NORM_ROWS = 16


def exchange_kernel(
    seqs,
    groups,
    local_heads,
    x_hbm,
    gain_ref,
    key_w_hbm,
    value_w_hbm,
    query_ref,
    offset_ref,
    key_out,
    value_out,
    read_ref,
    x_buf,
    normed,
    key_w,
    value_w,
    outgoing,
    arrived,
    group_read,
    group_rest,
    x_sem,
    w_sem,
    send_sem,
    recv_sem,
    out_sem,
):
    positions = x_buf.shape[1]
    width = x_buf.shape[2]
    columns = query_ref.shape[1]
    head_dim = columns // local_heads
    span = groups * positions
    pad = group_read.shape[1]
    my_seq = lax.axis_index("sp")
    my_group = lax.axis_index("tp")
    me = my_seq * groups + my_group
    upper = (my_seq >= seqs // 2).astype(jnp.int32)
    pair = (my_seq // 2) * 2

    quad = 4 if seqs % 4 == 0 else 1

    def seq_at(step):
        if quad == 1:
            return lax.rem(my_seq + 1 + step, seqs)
        jump = 2 * (step // 4) + lax.rem(step, 2)
        side = lax.rem(my_seq + lax.rem(step // 2, 2), 2)
        ahead = lax.rem(pair + 2 + 2 * jump, seqs)
        behind = lax.rem(pair - 2 - 2 * jump + 2 * seqs, seqs)
        return upper * behind + (1 - upper) * ahead + side

    def x_copy(step):
        seq = seq_at(step)
        return pltpu.make_async_copy(x_hbm.at[seq], x_buf.at[step], x_sem.at[step])

    def w_copy(index):
        cols = pl.ds(pl.multiple_of(index * columns, columns), columns)
        return (
            pltpu.make_async_copy(key_w_hbm.at[:, cols], key_w.at[index], w_sem.at[0, index]),
            pltpu.make_async_copy(value_w_hbm.at[:, cols], value_w.at[index], w_sem.at[1, index]),
        )

    def target(turn):
        turn = lax.rem(turn + my_seq // 2, groups)
        if groups % 2 == 0:
            turn = turn // 2 + lax.rem(turn, 2) * (groups // 2)
        return lax.rem(my_group + turn, groups)

    x_copy(jnp.int32(0)).start()
    for turn in range(groups):
        for copy in w_copy(target(jnp.int32(turn))):
            copy.start()
        if turn == 0 and seqs > 1:
            x_copy(jnp.int32(1)).start()

    @pl.loop(2, seqs)
    def _(step):
        x_copy(step).start()

    barrier = pltpu.get_barrier_semaphore()

    @pl.loop(0, seqs * groups)
    def _(device):
        @pl.when(device != me)
        def _():
            pl.semaphore_signal(
                barrier,
                inc=1,
                device_id=(device // groups, lax.rem(device, groups)),
                device_id_type=MESH,
            )

    def block_rows(device):
        return pl.ds(pl.multiple_of(device * positions, positions), positions)

    def remote(seq, group):
        device = seq * groups + group
        return pltpu.make_async_remote_copy(
            src_ref=outgoing.at[seq, group],
            dst_ref=arrived.at[block_rows(me)],
            send_sem=send_sem.at[device],
            recv_sem=recv_sem.at[me],
            device_id=(seq, group),
            device_id_type=MESH,
        )

    def own():
        return pltpu.make_async_copy(
            outgoing.at[my_seq, my_group], arrived.at[block_rows(me)], recv_sem.at[me]
        )

    def launch(seq, group):
        mine = seq * groups + group == me

        @pl.when(mine)
        def _():
            own().start()

        @pl.when(jnp.logical_not(mine))
        def _():
            remote(seq, group).start()

    def norm(step):
        x_copy(step).wait()
        slot = lax.rem(step, quad)

        @pl.loop(0, positions // NORM_ROWS)
        def _(chunk):
            rows = pl.ds(pl.multiple_of(chunk * NORM_ROWS, NORM_ROWS), NORM_ROWS)
            wide = x_buf[step, rows, :].astype(jnp.float32)
            scale = lax.rsqrt(jnp.sum(wide * wide, axis=-1, keepdims=True) / width + norm_epsilon)
            gain = gain_ref[...].astype(jnp.float32).reshape(1, width)
            normed[slot, rows, :] = (wide * scale * gain).astype(jnp.bfloat16)

    def project(step, turn):
        seq = seq_at(step)
        group = target(turn)
        slot = lax.rem(step, quad)
        outgoing[seq, group, :, :columns] = jnp.dot(
            normed[slot], key_w[group], preferred_element_type=jnp.float32
        ).astype(jnp.bfloat16)
        outgoing[seq, group, :, columns:] = jnp.dot(
            normed[slot], value_w[group], preferred_element_type=jnp.float32
        ).astype(jnp.bfloat16)

    def place(index):
        phase = index // (quad * groups)
        within = lax.rem(index, quad * groups)
        return phase * quad + lax.rem(within, quad), within // quad

    def launch_at(index):
        step, turn = place(index)
        launch(seq_at(step), target(turn))

    @pl.loop(0, seqs * groups)
    def _(index):
        step, turn = place(index)

        @pl.when(turn == 0)
        def _():
            norm(step)

        @pl.when(step == 0)
        def _():
            for copy in w_copy(target(turn)):
                copy.wait()

        project(step, turn)

        @pl.when(index == 0)
        def _():
            pl.semaphore_wait(barrier, seqs * groups - 1)

        @pl.when(index > 0)
        def _():
            launch_at(index - 1)

    row = lax.broadcasted_iota(jnp.int32, (pad, columns), 0)
    col = lax.broadcasted_iota(jnp.int32, (pad, columns), 1)
    query = jnp.where(
        row == col // head_dim,
        jnp.broadcast_to(query_ref[...].astype(jnp.float32), (pad, columns)),
        0.0,
    ).astype(jnp.bfloat16)
    launch_at(jnp.int32(seqs * groups - 1))

    score_row = lax.broadcasted_iota(jnp.int32, (pad, span), 0)
    score_col = lax.broadcasted_iota(jnp.int32, (pad, span), 1)
    offsets = jnp.zeros((pad, span), jnp.float32)
    for head in range(local_heads):
        offsets = jnp.where(score_row == head, offset_ref[my_group * local_heads + head], offsets)

    def out_copies(seq):
        rows = pl.ds(pl.multiple_of(seq * span, span), span)
        return (
            pltpu.make_async_copy(
                arrived.at[rows, pl.ds(0, columns)], key_out.at[rows], out_sem.at[0, seq]
            ),
            pltpu.make_async_copy(
                arrived.at[rows, pl.ds(columns, columns)], value_out.at[rows], out_sem.at[1, seq]
            ),
        )

    @pl.loop(0, seqs)
    def _(turn):
        seq = upper * (seqs - 1 - turn) + (1 - upper) * turn

        @pl.loop(0, groups)
        def _(group):
            device = seq * groups + group
            pltpu.make_async_copy(
                outgoing.at[seq, group], arrived.at[block_rows(device)], recv_sem.at[device]
            ).wait()

        for copy in out_copies(seq):
            copy.start()
        rows = pl.ds(pl.multiple_of(seq * span, span), span)
        scores = lax.dot_general(
            query,
            arrived[rows, :columns],
            (((1,), (1,)), ((), ())),
            preferred_element_type=jnp.float32,
        )
        scores = scores * head_dim ** (-0.5) + offsets
        soft = jnp.log1p(jnp.exp(-jnp.abs(scores)))
        rest = -jnp.maximum(scores, 0.0) - soft
        total = rest
        shift = 1
        while shift < span:
            total = total + jnp.where(
                score_col < span - shift, pltpu.roll(total, span - shift, 1), 0.0
            )
            shift *= 2
        later = total - rest
        weights = jnp.exp(jnp.minimum(scores, 0.0) - soft + later).astype(jnp.bfloat16)
        group_read[seq] = jnp.dot(
            weights, arrived[rows, columns:], preferred_element_type=jnp.float32
        )
        group_rest[seq] = jnp.broadcast_to(total[:, :1], (pad, columns))

    reading = jnp.zeros((pad, columns), jnp.float32)
    after = jnp.zeros((pad, columns), jnp.float32)
    for seq in reversed(range(seqs)):
        reading = reading + jnp.exp(after) * group_read[seq]
        after = after + group_rest[seq]
    for head in range(local_heads):
        own_cols = slice(head * head_dim, (head + 1) * head_dim)
        part = reading[head : head + 1, own_cols]
        read_ref[:, own_cols] = part * lax.rsqrt(
            jnp.mean(part * part, axis=-1, keepdims=True) + norm_epsilon
        )

    @pl.loop(0, seqs * groups)
    def _(device):
        @pl.when(device != me)
        def _():
            remote(device // groups, lax.rem(device, groups)).wait_send()

    @pl.loop(0, seqs)
    def _(seq):
        for copy in out_copies(seq):
            copy.wait()


def shards(seqs, groups, layer_input, norm_gain, key_weight, value_weight, new_query, score_offset):
    seq_count, positions, width = layer_input.shape
    columns = new_query.shape[1]
    local_heads = score_offset.shape[0] // groups
    pad = -(-local_heads // 8) * 8
    length = seqs * groups * positions
    any_space = pl.BlockSpec(memory_space=pl.ANY)
    vmem = pl.BlockSpec(memory_space=pltpu.VMEM)
    keys, values, read = pl.pallas_call(
        functools.partial(exchange_kernel, seqs, groups, local_heads),
        out_shape=(
            pltpu.VMEM((length, columns), jnp.bfloat16),
            pltpu.VMEM((length, columns), jnp.bfloat16),
            jax.ShapeDtypeStruct((1, columns), jnp.float32),
        ),
        in_specs=[
            any_space,
            vmem,
            any_space,
            any_space,
            vmem,
            pl.BlockSpec(memory_space=pltpu.SMEM),
        ],
        out_specs=(vmem, vmem, vmem),
        scratch_shapes=[
            pltpu.VMEM((seq_count, positions, width), jnp.bfloat16),
            pltpu.VMEM((4 if seqs % 4 == 0 else 1, positions, width), jnp.bfloat16),
            pltpu.VMEM((groups, width, columns), jnp.bfloat16),
            pltpu.VMEM((groups, width, columns), jnp.bfloat16),
            pltpu.VMEM((seqs, groups, positions, 2 * columns), jnp.bfloat16),
            pltpu.VMEM((length, 2 * columns), jnp.bfloat16),
            pltpu.VMEM((seqs, pad, columns), jnp.float32),
            pltpu.VMEM((seqs, pad, columns), jnp.float32),
            pltpu.SemaphoreType.DMA((seq_count,)),
            pltpu.SemaphoreType.DMA((2, groups)),
            pltpu.SemaphoreType.DMA((seqs * groups,)),
            pltpu.SemaphoreType.DMA((seqs * groups,)),
            pltpu.SemaphoreType.DMA((2, seqs)),
        ],
        compiler_params=pltpu.CompilerParams(
            collective_id=0, has_side_effects=True, vmem_limit_bytes=50000000
        ),
    )(layer_input, norm_gain, key_weight, value_weight, new_query, score_offset)
    return (keys[None], values[None], read)


def solution(mesh):
    seqs = mesh.shape["sp"]
    groups = mesh.shape["tp"]
    placed = (P(None, ("sp", "tp"), None), P(), P(), P(), P("sp", "tp"), P())
    return jax.shard_map(
        functools.partial(shards, seqs, groups),
        mesh=mesh,
        in_specs=placed,
        out_specs=(P("sp", None, "tp"), P("sp", None, "tp"), P("sp", "tp")),
        check_vma=False,
    )
```

profile of v0, /device:TPU:0, one launch (start us, length us, event | category | flops | bytes accessed | tf_op | source)
XLA Modules:
  0.0 112.8 jit_solution(5782767688503112973)
XLA Ops:
  0.6 0.0 copy-start
  0.6 0.7 copy-done
  1.3 0.0 copy-start.1
  1.3 0.7 copy-done.1
  2.0 0.0 copy-start.2
  2.0 0.7 copy-done.2
  2.7 106.9 %shard_map.85 = (bf16[4096,256]{1,0:T(8,128)(2,1)S(1)}, bf16[4096,256]{1,0:T(8,128)(2,1)S(1)}, f32[1,256]{1,0:T(1,128)S(1)}) custom-call(bf16[8,128,2048]{2,1,0:T(8,128)(2,1)} %x_hbm.1, bf16[2048]{0:T(1024)(128)(2,1)S(1)} %copy-done, bf16[2048,1024]{1,0:T(8,128)(2,1)} %key_w_hbm.1, bf16[2048,1024]{1,0:T(8,128)(2,1)} %value_w_hbm.1, ...), custom_call_target="tpu_custom_call" | custom-call | tf_op jit(solution)/shard_map/pallas_call | solution.py:286
  109.6 1.3 %copy.12 = bf16[1,4096,256]{2,1,0:T(8,128)(2,1)} copy(bf16[1,4096,256]{2,1,0:T(8,128)(2,1)S(1)} %bitcast.3) | data formatting | bytes 4194304
  110.9 1.3 %copy.13 = bf16[1,4096,256]{2,1,0:T(8,128)(2,1)} copy(bf16[1,4096,256]{2,1,0:T(8,128)(2,1)S(1)} %bitcast.2) | data formatting | bytes 4194304
  112.2 0.6 copy.14
Async XLA Ops:
  0.6 0.7 copy-start
  1.3 0.7 copy-start.1
  2.0 0.7 copy-start.2
where the time goes:
time: 113 us
  Pallas kernels  107 us (95%)
  local copies, waits for them, and re-layouts  5.21 us (5%)
    pallas_call x1, Pallas kernels, shards(): pl.pallas_call(functools.partial(exchange_kernel, seqs, groups, local_hea...  107 us
    unnamed x9, local copies, waits for them, and re-layouts  5.21 us

commit v1 on v0

v1 whole, which is shorter than its diff:
```python
import functools

import jax
import jax.numpy as jnp
from jax import lax
from jax.experimental import pallas as pl
from jax.experimental.pallas import tpu as pltpu
from jax.sharding import PartitionSpec as P

norm_epsilon = 1e-06
MESH = pl.DeviceIdType.MESH
NORM_ROWS = 16
BATCH = 4
VMEM_BYTES = 64000000


class Layout:
    def __init__(self, seqs, groups):
        self.seqs = seqs
        self.groups = groups
        self.sides = 2 if seqs % 2 == 0 else 1
        self.cores = 2 if groups % 2 == 0 else 1
        self.planes = seqs // self.sides
        self.ranks = groups // self.cores
        self.per_plane = self.sides * groups
        seq = lax.axis_index("sp")
        group = lax.axis_index("tp")
        self.me = seq * groups + group
        self.seq = seq
        self.group = group
        self.side = lax.rem(seq, self.sides)
        self.plane = seq // self.sides
        self.core = lax.rem(group, self.cores)
        self.rank = group // self.cores
        self.upper = (2 * self.plane >= self.planes).astype(jnp.int32)

    def far_plane(self, step):
        return self.upper * step + (1 - self.upper) * (self.planes - 1 - step)

    def send_seq(self, half):
        side = lax.rem(self.side + half + self.core, self.sides)
        return self.far_plane(half // self.sides) * self.sides + side

    def send_group(self, turn):
        rank = lax.rem(self.rank + turn // self.cores, self.ranks)
        return rank * self.cores + lax.rem(self.core + turn, self.cores)

    def source_plane(self, step):
        near = self.planes - self.planes // 2
        plane = self.upper * (self.planes - 1 - self.plane) + (1 - self.upper) * self.plane
        first = lax.rem(plane + step, near)
        later = self.planes - 1 - (step - near)
        is_near = (step < near).astype(jnp.int32)
        plane = is_near * first + (1 - is_near) * later
        return self.upper * (self.planes - 1 - plane) + (1 - self.upper) * plane

    def source(self, index):
        within = lax.rem(index, self.per_plane)
        turn = lax.rem(within, self.groups)
        core = lax.rem(self.core + self.cores - lax.rem(turn, self.cores), self.cores)
        flip = lax.rem(within // self.groups + core, self.sides)
        side = lax.rem(self.side + self.sides - flip, self.sides)
        rank = lax.rem(self.rank + self.ranks - turn // self.cores, self.ranks)
        plane = self.source_plane(index // self.per_plane)
        return (plane * self.sides + side) * self.groups + rank * self.cores + core


def read_block(query, offsets, earlier, keys, values, head_dim):
    scores = lax.dot_general(
        query, keys, (((1,), (1,)), ((), ())), preferred_element_type=jnp.float32
    )
    scores = scores * head_dim ** (-0.5) + offsets
    soft = jnp.log1p(jnp.exp(-jnp.abs(scores)))
    rest = -jnp.maximum(scores, 0.0) - soft
    positions = scores.shape[1]
    sums = jnp.zeros((scores.shape[0], 2 * positions), jnp.float32)
    left = rest
    for _ in range(3):
        piece = left.astype(jnp.bfloat16)
        left = left - piece.astype(jnp.float32)
        sums = sums + jnp.dot(piece, earlier, preferred_element_type=jnp.float32)
    later = sums[:, :positions]
    weights = jnp.exp(jnp.minimum(scores, 0.0) - soft + later).astype(jnp.bfloat16)
    reading = jnp.dot(weights, values, preferred_element_type=jnp.float32)
    return reading, sums[:, positions:]


def later_matrix(positions):
    row = lax.broadcasted_iota(jnp.int32, (positions, 2 * positions), 0)
    col = lax.broadcasted_iota(jnp.int32, (positions, 2 * positions), 1)
    return ((row > col) | (col >= positions)).astype(jnp.float32).astype(jnp.bfloat16)


def exchange_kernel(
    seqs,
    groups,
    local_heads,
    x_hbm,
    gain_hbm,
    key_w_hbm,
    value_w_hbm,
    query_hbm,
    offset_hbm,
    arrived,
    block_read,
    block_rest,
    masked_query,
    offsets,
    x_buf,
    gain,
    query,
    offset,
    normed,
    key_w,
    value_w,
    outgoing,
    x_sem,
    w_sem,
    small_sem,
    send_sem,
    recv_sem,
):
    positions = x_buf.shape[1]
    width = x_buf.shape[2]
    columns = query.shape[1]
    head_dim = columns // local_heads
    pad = masked_query.shape[0]
    devices = seqs * groups
    at = Layout(seqs, groups)
    me = at.me

    def x_copy(half):
        return pltpu.make_async_copy(x_hbm.at[at.send_seq(half)], x_buf.at[half], x_sem.at[half])

    def w_copy(turn, part):
        group = at.send_group(turn)
        cols = pl.ds(pl.multiple_of(group * columns, columns), columns)
        source = (key_w_hbm, value_w_hbm)[part].at[:, cols]
        return pltpu.make_async_copy(source, (key_w, value_w)[part].at[turn], w_sem.at[part, turn])

    small_copies = (
        pltpu.make_async_copy(gain_hbm, gain, small_sem.at[0]),
        pltpu.make_async_copy(query_hbm, query, small_sem.at[1]),
        pltpu.make_async_copy(offset_hbm, offset, small_sem.at[2]),
    )

    barrier = pltpu.get_barrier_semaphore()

    @pl.loop(0, devices)
    def _(device):
        @pl.when(device != me)
        def _():
            pl.semaphore_signal(
                barrier,
                inc=1,
                device_id=(device // groups, lax.rem(device, groups)),
                device_id_type=MESH,
            )

    x_copy(0).start()
    for copy in small_copies:
        copy.start()
    for turn in range(groups):
        w_copy(turn, 0).start()
        w_copy(turn, 1).start()
        if turn == 0 and seqs > 1:
            x_copy(1).start()

    @pl.loop(2, seqs)
    def _(half):
        x_copy(half).start()

    def block_rows(device):
        return pl.ds(pl.multiple_of(device * positions, positions), positions)

    def remote(half, turn, part):
        seq = at.send_seq(half)
        group = at.send_group(turn)
        device = seq * groups + group
        cols = pl.ds(part * columns, columns)
        return device, pltpu.make_async_remote_copy(
            src_ref=outgoing.at[half, turn, :, cols],
            dst_ref=arrived.at[block_rows(me), cols],
            send_sem=send_sem.at[device],
            recv_sem=recv_sem.at[me],
            device_id=(seq, group),
            device_id_type=MESH,
        )

    def launch(half, turn, part):
        device, copy = remote(half, turn, part)

        @pl.when(device != me)
        def _():
            copy.start()

        @pl.when(device == me)
        def _():
            cols = slice(part * columns, (part + 1) * columns)
            arrived[block_rows(me), cols] = outgoing[half, turn, :, cols]

    def norm(half):
        x_copy(half).wait()

        @pl.loop(0, positions // NORM_ROWS)
        def _(chunk):
            rows = pl.ds(pl.multiple_of(chunk * NORM_ROWS, NORM_ROWS), NORM_ROWS)
            wide = x_buf[half, rows, :].astype(jnp.float32)
            scale = lax.rsqrt(jnp.sum(wide * wide, axis=-1, keepdims=True) / width + norm_epsilon)
            normed[rows, :] = (wide * scale * gain[...].astype(jnp.float32).reshape(1, width)).astype(
                jnp.bfloat16
            )

    def project(half, turn, part):
        weight = (key_w, value_w)[part]
        outgoing[half, turn, :, part * columns : (part + 1) * columns] = jnp.dot(
            normed[...], weight[turn], preferred_element_type=jnp.float32
        ).astype(jnp.bfloat16)

    small_copies[0].wait()

    @pl.loop(0, devices)
    def _(index):
        half = index // groups
        turn = lax.rem(index, groups)

        @pl.when(turn == 0)
        def _():
            norm(half)

        @pl.when(half == 0)
        def _():
            w_copy(turn, 0).wait()

        project(half, turn, 0)

        @pl.when(index == 0)
        def _():
            pl.semaphore_wait(barrier, devices - 1)

        @pl.when(index > 0)
        def _():
            launch((index - 1) // groups, lax.rem(index - 1, groups), 1)

        @pl.when(half == 0)
        def _():
            w_copy(turn, 1).wait()

        project(half, turn, 1)
        launch(half, turn, 0)

    small_copies[1].wait()
    small_copies[2].wait()
    row = lax.broadcasted_iota(jnp.int32, (pad, columns), 0)
    col = lax.broadcasted_iota(jnp.int32, (pad, columns), 1)
    masked_query[...] = jnp.where(
        row == col // head_dim,
        jnp.broadcast_to(query[...].astype(jnp.float32), (pad, columns)),
        0.0,
    ).astype(jnp.bfloat16)
    score_row = lax.broadcasted_iota(jnp.int32, (pad, positions), 0)
    head_offsets = jnp.zeros((pad, positions), jnp.float32)
    for head in range(local_heads):
        head_offsets = jnp.where(
            score_row == head, offset[at.group * local_heads + head], head_offsets
        )
    offsets[...] = head_offsets
    launch(seqs - 1, groups - 1, 1)

    earlier = later_matrix(positions)

    def wait_block(source):
        @pl.when(source != me)
        def _():
            pltpu.make_async_copy(
                outgoing.at[0, 0], arrived.at[block_rows(source)], recv_sem.at[source]
            ).wait()

    @pl.loop(0, devices // BATCH)
    def _(batch):
        sources = [at.source(batch * BATCH + k) for k in range(BATCH)]
        for source in sources:
            wait_block(source)

        @pl.when(batch < devices // BATCH - 1)
        def _():
            for source in sources:
                rows = block_rows(source)
                reading, rest = read_block(
                    masked_query[...],
                    offsets[...],
                    earlier,
                    arrived[rows, :columns],
                    arrived[rows, columns:],
                    head_dim,
                )
                block_read[source] = reading
                block_rest[source] = rest

    @pl.loop(0, devices)
    def _(index):
        half = index // groups
        turn = lax.rem(index, groups)
        device = at.send_seq(half) * groups + at.send_group(turn)

        @pl.when(device != me)
        def _():
            pltpu.make_async_copy(
                outgoing.at[half, turn], arrived.at[block_rows(device)], send_sem.at[device]
            ).wait()


def finish_kernel(
    seqs,
    groups,
    local_heads,
    arrived,
    block_read,
    block_rest,
    masked_query,
    offsets,
    keys_hbm,
    values_hbm,
    read_hbm,
    last_read,
    last_rest,
    read,
    out_sem,
    read_sem,
):
    devices = seqs * groups
    length = arrived.shape[0]
    positions = length // devices
    columns = masked_query.shape[1]
    head_dim = columns // local_heads
    at = Layout(seqs, groups)
    pieces = out_sem.shape[1]
    span = length // pieces

    def out_copies(piece):
        rows = pl.ds(piece * span, span)
        return (
            pltpu.make_async_copy(
                arrived.at[rows, pl.ds(0, columns)], keys_hbm.at[rows], out_sem.at[0, piece]
            ),
            pltpu.make_async_copy(
                arrived.at[rows, pl.ds(columns, columns)], values_hbm.at[rows], out_sem.at[1, piece]
            ),
        )

    for piece in range(pieces):
        for copy in out_copies(piece):
            copy.start()

    sources = [at.source(jnp.int32(devices - BATCH + k)) for k in range(BATCH)]
    earlier = later_matrix(positions)
    last_read[...] = block_read[...]
    last_rest[...] = block_rest[...]
    for source in sources:
        rows = pl.ds(pl.multiple_of(source * positions, positions), positions)
        reading, rest = read_block(
            masked_query[...],
            offsets[...],
            earlier,
            arrived[rows, :columns],
            arrived[rows, columns:],
            head_dim,
        )
        last_read[source] = reading
        last_rest[source] = rest

    reading = jnp.zeros(last_read.shape[1:], jnp.float32)
    after = jnp.zeros(last_rest.shape[1:], jnp.float32)
    for device in reversed(range(devices)):
        scale = jnp.exp(after)
        reading = reading + jnp.concatenate([scale] * (columns // positions), axis=1) * last_read[device]
        after = after + last_rest[device]
    for head in range(local_heads):
        own_cols = slice(head * head_dim, (head + 1) * head_dim)
        part = reading[head : head + 1, own_cols]
        read[:, own_cols] = part * lax.rsqrt(
            jnp.mean(part * part, axis=-1, keepdims=True) + norm_epsilon
        )
    read_copy = pltpu.make_async_copy(read, read_hbm, read_sem)
    read_copy.start()
    for piece in range(pieces):
        for copy in out_copies(piece):
            copy.wait()
    read_copy.wait()


def shards(seqs, groups, layer_input, norm_gain, key_weight, value_weight, new_query, score_offset):
    seq_count, positions, width = layer_input.shape
    columns = new_query.shape[1]
    local_heads = score_offset.shape[0] // groups
    pad = -(-local_heads // 8) * 8
    devices = seqs * groups
    length = devices * positions
    hbm = pl.BlockSpec(memory_space=pltpu.HBM)
    vmem = pl.BlockSpec(memory_space=pltpu.VMEM)
    passed_bytes = 4 * length * columns + 4 * devices * pad * (columns + positions)
    passed = pl.pallas_call(
        functools.partial(exchange_kernel, seqs, groups, local_heads),
        out_shape=(
            pltpu.VMEM((length, 2 * columns), jnp.bfloat16),
            pltpu.VMEM((devices, pad, columns), jnp.float32),
            pltpu.VMEM((devices, pad, positions), jnp.float32),
            pltpu.VMEM((pad, columns), jnp.bfloat16),
            pltpu.VMEM((pad, positions), jnp.float32),
        ),
        in_specs=[hbm] * 6,
        out_specs=(vmem,) * 5,
        scratch_shapes=[
            pltpu.VMEM((seq_count, positions, width), jnp.bfloat16),
            pltpu.VMEM((width,), jnp.bfloat16),
            pltpu.VMEM((1, columns), jnp.bfloat16),
            pltpu.SMEM(score_offset.shape, jnp.float32),
            pltpu.VMEM((positions, width), jnp.bfloat16),
            pltpu.VMEM((groups, width, columns), jnp.bfloat16),
            pltpu.VMEM((groups, width, columns), jnp.bfloat16),
            pltpu.VMEM((seqs, groups, positions, 2 * columns), jnp.bfloat16),
            pltpu.SemaphoreType.DMA((seq_count,)),
            pltpu.SemaphoreType.DMA((2, groups)),
            pltpu.SemaphoreType.DMA((3,)),
            pltpu.SemaphoreType.DMA((devices,)),
            pltpu.SemaphoreType.DMA((devices,)),
        ],
        compiler_params=pltpu.CompilerParams(
            collective_id=0, has_side_effects=True, vmem_limit_bytes=VMEM_BYTES - passed_bytes
        ),
    )(layer_input, norm_gain, key_weight, value_weight, new_query, score_offset)
    keys, values, read = pl.pallas_call(
        functools.partial(finish_kernel, seqs, groups, local_heads),
        out_shape=(
            jax.ShapeDtypeStruct((length, columns), jnp.bfloat16),
            jax.ShapeDtypeStruct((length, columns), jnp.bfloat16),
            jax.ShapeDtypeStruct((1, columns), jnp.float32),
        ),
        in_specs=[vmem] * 5,
        out_specs=(hbm,) * 3,
        scratch_shapes=[
            pltpu.VMEM((devices, pad, columns), jnp.float32),
            pltpu.VMEM((devices, pad, positions), jnp.float32),
            pltpu.VMEM((1, columns), jnp.float32),
            pltpu.SemaphoreType.DMA((2, 4)),
            pltpu.SemaphoreType.DMA,
        ],
        compiler_params=pltpu.CompilerParams(vmem_limit_bytes=20000000),
    )(*passed)
    return (keys[None], values[None], read)


def solution(mesh):
    seqs = mesh.shape["sp"]
    groups = mesh.shape["tp"]
    placed = (P(None, ("sp", "tp"), None), P(), P(), P(), P("sp", "tp"), P())
    return jax.shard_map(
        functools.partial(shards, seqs, groups),
        mesh=mesh,
        in_specs=placed,
        out_specs=(P("sp", None, "tp"), P("sp", None, "tp"), P("sp", "tp")),
        check_vma=False,
    )
```

time: 113 us -> 105 us (0.929)
  the two profiles are of different devices: /device:TPU:0 before, /device:TPU:13 now
where the time goes in v1:
time: 105 us; the launch traced here: 103 us
  Pallas kernels  103 us (98%)
    pallas_call x1, Pallas kernels, shards(): pl.pallas_call(functools.partial(exchange_kernel, seqs, groups, local_hea...  100 us
    pallas_call x1, Pallas kernels, shards(): pl.pallas_call(functools.partial(finish_kernel, seqs, groups, local_heads...  2.82 us

profile of v1, /device:TPU:13, one launch (start us, length us, event | category | flops | bytes accessed | tf_op | source)
XLA Modules:
  0.0 103.5 jit_solution(8793668058683218728)
XLA Ops:
  0.6 100.0 %shard_map.85 = (bf16[4096,512]{1,0:T(8,128)(2,1)S(1)}, f32[32,8,256]{2,1,0:T(8,128)S(1)}, f32[32,8,128]{2,1,0:T(8,128)S(1)}, bf16[8,256]{1,0:T(8,128)(2,1)S(1)}, f32[8,128]{1,0:T(8,128)S(1)}) custom-call(bf16[8,128,2048]{2,1,0:T(8,128)(2,1)} %x_hbm.1, bf16[2048]{0:T(1024)(128)(2,1)} %gain_hbm.1, bf16[2048,1024]{1,0:T(8,128)(2,1)} %key_w_hbm.1, ...), custom_call_target="tpu_custom_call" | custom-call | tf_op jit(solution)/shard_map/pallas_call | solution.py:402
  100.6 2.8 %shard_map.86 = (bf16[4096,256]{1,0:T(8,128)(2,1)}, bf16[4096,256]{1,0:T(8,128)(2,1)}, f32[1,256]{1,0:T(1,128)}) custom-call(bf16[4096,512]{1,0:T(8,128)(2,1)S(1)} %get-tuple-element.11.arrived, f32[32,8,256]{2,1,0:T(8,128)S(1)} %get-tuple-element.12.block_read, f32[32,8,128]{2,1,0:T(8,128)S(1)} %get-tuple-element.13.block_rest, ...), custom_call_target="tpu_custom_call" | custom-call | tf_op jit(solution)/shard_map/pallas_call | solution.py:432

commit v2 on v1

--- a/solution.py
+++ b/solution.py
@@ -9,8 +9,10 @@
 
 norm_epsilon = 1e-06
 MESH = pl.DeviceIdType.MESH
-NORM_ROWS = 16
+NORM_ROWS = 64
+LANES = 128
 BATCH = 4
+EARLY = 2
 VMEM_BYTES = 64000000
 
 
@@ -40,6 +42,19 @@
     def send_seq(self, half):
         side = lax.rem(self.side + half + self.core, self.sides)
         return self.far_plane(half // self.sides) * self.sides + side
+
+    def near_half(self):
+        if self.planes == 1:
+            return jnp.int32(0)
+        step = self.upper * (self.plane - 1) + (1 - self.upper) * (self.planes - 2 - self.plane)
+        return step * self.sides
+
+    def place(self, index):
+        first = self.near_half() * self.groups
+        late = index - EARLY
+        late = late + EARLY * (late >= first).astype(jnp.int32)
+        number = jnp.where(index < EARLY, first + index, late)
+        return number // self.groups, lax.rem(number, self.groups)
 
     def send_group(self, turn):
         rank = lax.rem(self.rank + turn // self.cores, self.ranks)
@@ -119,6 +134,7 @@
     small_sem,
     send_sem,
     recv_sem,
+    round_sem,
 ):
     positions = x_buf.shape[1]
     width = x_buf.shape[2]
@@ -145,9 +161,33 @@
     )
 
     barrier = pltpu.get_barrier_semaphore()
-
-    @pl.loop(0, devices)
-    def _(device):
+    below = (at.plane > 0).astype(jnp.int32)
+    above = (at.plane < at.planes - 1).astype(jnp.int32)
+
+    def signal_column(semaphore):
+        @pl.when(below == 1)
+        def _():
+            pl.semaphore_signal(
+                semaphore, inc=1, device_id=(at.seq - at.sides, at.group), device_id_type=MESH
+            )
+
+        @pl.when(above == 1)
+        def _():
+            pl.semaphore_signal(
+                semaphore, inc=1, device_id=(at.seq + at.sides, at.group), device_id_type=MESH
+            )
+
+    near = at.near_half()
+    x_copy(near).start()
+    small_copies[0].start()
+    w_copy(0, 0).start()
+    w_copy(0, 1).start()
+    signal_column(barrier)
+
+    @pl.loop(0, at.per_plane)
+    def _(peer):
+        device = at.plane * at.per_plane + peer
+
         @pl.when(device != me)
         def _():
             pl.semaphore_signal(
@@ -157,18 +197,31 @@
                 device_id_type=MESH,
             )
 
-    x_copy(0).start()
-    for copy in small_copies:
-        copy.start()
-    for turn in range(groups):
+    x_copy(near).wait()
+    small_copies[0].wait()
+    for turn in range(1, groups):
         w_copy(turn, 0).start()
         w_copy(turn, 1).start()
-        if turn == 0 and seqs > 1:
-            x_copy(1).start()
-
-    @pl.loop(2, seqs)
+    small_copies[1].start()
+    small_copies[2].start()
+
+    @pl.loop(0, seqs)
     def _(half):
-        x_copy(half).start()
+        @pl.when(half != near)
+        def _():
+            x_copy(half).start()
+
+    rounds = at.planes - 1
+    if rounds == 0:
+        pl.semaphore_wait(barrier, at.per_plane - 1)
+    else:
+        pl.semaphore_wait(barrier, at.per_plane - 1 + below + above)
+        signal_column(round_sem.at[0])
+
+    def finish_round(number):
+        pl.semaphore_wait(round_sem.at[number], below + above)
+        if number + 1 < rounds:
+            signal_column(round_sem.at[number + 1])
 
     def block_rows(device):
         return pl.ds(pl.multiple_of(device * positions, positions), positions)
@@ -200,16 +253,20 @@
             arrived[block_rows(me), cols] = outgoing[half, turn, :, cols]
 
     def norm(half):
-        x_copy(half).wait()
-
         @pl.loop(0, positions // NORM_ROWS)
         def _(chunk):
             rows = pl.ds(pl.multiple_of(chunk * NORM_ROWS, NORM_ROWS), NORM_ROWS)
-            wide = x_buf[half, rows, :].astype(jnp.float32)
-            scale = lax.rsqrt(jnp.sum(wide * wide, axis=-1, keepdims=True) / width + norm_epsilon)
-            normed[rows, :] = (wide * scale * gain[...].astype(jnp.float32).reshape(1, width)).astype(
-                jnp.bfloat16
-            )
+            squares = jnp.zeros((NORM_ROWS, LANES), jnp.float32)
+            for first in range(0, width, LANES):
+                wide = x_buf[half, rows, first : first + LANES].astype(jnp.float32)
+                squares = squares + wide * wide
+            scale = lax.rsqrt(jnp.sum(squares, axis=-1, keepdims=True) / width + norm_epsilon)
+            for first in range(0, width, LANES):
+                cols = slice(first, first + LANES)
+                wide = x_buf[half, rows, cols].astype(jnp.float32)
+                normed[rows, cols] = (
+                    wide * scale * gain[cols].astype(jnp.float32).reshape(1, LANES)
+                ).astype(jnp.bfloat16)
 
     def project(half, turn, part):
         weight = (key_w, value_w)[part]
@@ -217,36 +274,42 @@
             normed[...], weight[turn], preferred_element_type=jnp.float32
         ).astype(jnp.bfloat16)
 
-    small_copies[0].wait()
-
     @pl.loop(0, devices)
     def _(index):
-        half = index // groups
-        turn = lax.rem(index, groups)
-
-        @pl.when(turn == 0)
+        half, turn = at.place(index)
+
+        @pl.when((turn == 0) & (half != near))
+        def _():
+            x_copy(half).wait()
+
+        @pl.when((turn == 0) | (index == EARLY) | ((half == near) & (turn == EARLY)))
         def _():
             norm(half)
 
-        @pl.when(half == 0)
+        fresh = (index < EARLY) | ((index < EARLY + groups) & (turn >= EARLY))
+
+        @pl.when(fresh)
         def _():
             w_copy(turn, 0).wait()
 
         project(half, turn, 0)
 
-        @pl.when(index == 0)
-        def _():
-            pl.semaphore_wait(barrier, devices - 1)
-
         @pl.when(index > 0)
         def _():
-            launch((index - 1) // groups, lax.rem(index - 1, groups), 1)
-
-        @pl.when(half == 0)
+            last_half, last_turn = at.place(index - 1)
+            launch(last_half, last_turn, 1)
+
+        @pl.when(fresh)
         def _():
             w_copy(turn, 1).wait()
 
         project(half, turn, 1)
+        for number in range(rounds):
+
+            @pl.when(index == min(number, EARLY))
+            def _():
+                finish_round(number)
+
         launch(half, turn, 0)
 
     small_copies[1].wait()
@@ -265,7 +328,8 @@
             score_row == head, offset[at.group * local_heads + head], head_offsets
         )
     offsets[...] = head_offsets
-    launch(seqs - 1, groups - 1, 1)
+    last_half, last_turn = at.place(jnp.int32(devices - 1))
+    launch(last_half, last_turn, 1)
 
     earlier = later_matrix(positions)
 
@@ -276,26 +340,23 @@
                 outgoing.at[0, 0], arrived.at[block_rows(source)], recv_sem.at[source]
             ).wait()
 
-    @pl.loop(0, devices // BATCH)
+    @pl.loop(0, devices // BATCH - 1)
     def _(batch):
         sources = [at.source(batch * BATCH + k) for k in range(BATCH)]
         for source in sources:
             wait_block(source)
-
-        @pl.when(batch < devices // BATCH - 1)
-        def _():
-            for source in sources:
-                rows = block_rows(source)
-                reading, rest = read_block(
-                    masked_query[...],
-                    offsets[...],
-                    earlier,
-                    arrived[rows, :columns],
-                    arrived[rows, columns:],
-                    head_dim,
-                )
-                block_read[source] = reading
-                block_rest[source] = rest
+        for source in sources:
+            rows = block_rows(source)
+            reading, rest = read_block(
+                masked_query[...],
+                offsets[...],
+                earlier,
+                arrived[rows, :columns],
+                arrived[rows, columns:],
+                head_dim,
+            )
+            block_read[source] = reading
+            block_rest[source] = rest
 
     @pl.loop(0, devices)
     def _(index):
@@ -308,6 +369,9 @@
             pltpu.make_async_copy(
                 outgoing.at[half, turn], arrived.at[block_rows(device)], send_sem.at[device]
             ).wait()
+
+    for k in range(BATCH):
+        wait_block(at.source(jnp.int32(devices - BATCH + k)))
 
 
 def finish_kernel(
@@ -382,7 +446,7 @@
             jnp.mean(part * part, axis=-1, keepdims=True) + norm_epsilon
         )
     read_copy = pltpu.make_async_copy(read, read_hbm, read_sem)
-    read_copy.start()
+    read_copy.start(priority=1)
     for piece in range(pieces):
         for copy in out_copies(piece):
             copy.wait()
@@ -424,6 +488,7 @@
             pltpu.SemaphoreType.DMA((3,)),
             pltpu.SemaphoreType.DMA((devices,)),
             pltpu.SemaphoreType.DMA((devices,)),
+            pltpu.SemaphoreType.REGULAR((seqs,)),
         ],
         compiler_params=pltpu.CompilerParams(
             collective_id=0, has_side_effects=True, vmem_limit_bytes=VMEM_BYTES - passed_bytes

time: 105 us -> 102 us (0.971)
  Pallas kernels: 103 us -> 100 us
    pallas_call x1, Pallas kernels: 100 us -> 97.2 us  [shards(): pl.pallas_call(functools.partial(exchange_kernel, seqs, groups, local_hea...]
where the time goes in v2:
time: 102 us; the launch traced here: 101 us
  Pallas kernels  100 us (98%)
    pallas_call x1, Pallas kernels, shards(): pl.pallas_call(functools.partial(exchange_kernel, seqs, groups, local_hea...  97.2 us
    pallas_call x1, Pallas kernels, shards(): pl.pallas_call(functools.partial(finish_kernel, seqs, groups, local_heads...  2.82 us

profile of v2, /device:TPU:13, one launch (start us, length us, event | category | flops | bytes accessed | tf_op | source)
XLA Modules:
  0.0 100.6 jit_solution(4112017795745666166)
XLA Ops:
  0.6 97.2 %shard_map.85 = (bf16[4096,512]{1,0:T(8,128)(2,1)S(1)}, f32[32,8,256]{2,1,0:T(8,128)S(1)}, f32[32,8,128]{2,1,0:T(8,128)S(1)}, bf16[8,256]{1,0:T(8,128)(2,1)S(1)}, f32[8,128]{1,0:T(8,128)S(1)}) custom-call(bf16[8,128,2048]{2,1,0:T(8,128)(2,1)} %x_hbm.1, bf16[2048]{0:T(1024)(128)(2,1)} %gain_hbm.1, bf16[2048,1024]{1,0:T(8,128)(2,1)} %key_w_hbm.1, ...), custom_call_target="tpu_custom_call" | custom-call | tf_op jit(solution)/shard_map/pallas_call | solution.py:466
  97.8 2.8 %shard_map.86 = (bf16[4096,256]{1,0:T(8,128)(2,1)}, bf16[4096,256]{1,0:T(8,128)(2,1)}, f32[1,256]{1,0:T(1,128)}) custom-call(bf16[4096,512]{1,0:T(8,128)(2,1)S(1)} %get-tuple-element.11.arrived, f32[32,8,256]{2,1,0:T(8,128)S(1)} %get-tuple-element.12.block_read, f32[32,8,128]{2,1,0:T(8,128)S(1)} %get-tuple-element.13.block_rest, ...), custom_call_target="tpu_custom_call" | custom-call | tf_op jit(solution)/shard_map/pallas_call | solution.py:497

commit v3 on v2

--- a/solution.py
+++ b/solution.py
@@ -13,6 +13,7 @@
 LANES = 128
 BATCH = 4
 EARLY = 2
+LAG = 2
 VMEM_BYTES = 64000000
 
 
@@ -35,6 +36,10 @@
         self.core = lax.rem(group, self.cores)
         self.rank = group // self.cores
         self.upper = (2 * self.plane >= self.planes).astype(jnp.int32)
+        self.inner = self.plane + 1 - 2 * self.upper
+        self.outer = self.plane - 1 + 2 * self.upper
+        self.has_outer = (self.outer >= 0) & (self.outer < self.planes)
+        self.is_middle = (2 * self.inner >= self.planes) != (self.upper == 1)
 
     def far_plane(self, step):
         return self.upper * step + (1 - self.upper) * (self.planes - 1 - step)
@@ -44,10 +49,13 @@
         return self.far_plane(half // self.sides) * self.sides + side
 
     def near_half(self):
-        if self.planes == 1:
-            return jnp.int32(0)
-        step = self.upper * (self.plane - 1) + (1 - self.upper) * (self.planes - 2 - self.plane)
-        return step * self.sides
+        step = jnp.int32(0)
+        if self.planes > 1:
+            step = self.upper * (self.plane - 1) + (1 - self.upper) * (self.planes - 2 - self.plane)
+        return step * self.sides + self.straight()
+
+    def straight(self):
+        return lax.rem(self.sides - self.core, self.sides)
 
     def place(self, index):
         first = self.near_half() * self.groups
@@ -161,42 +169,95 @@
     )
 
     barrier = pltpu.get_barrier_semaphore()
-    below = (at.plane > 0).astype(jnp.int32)
-    above = (at.plane < at.planes - 1).astype(jnp.int32)
-
-    def signal_column(semaphore):
-        @pl.when(below == 1)
-        def _():
-            pl.semaphore_signal(
-                semaphore, inc=1, device_id=(at.seq - at.sides, at.group), device_id_type=MESH
-            )
-
-        @pl.when(above == 1)
-        def _():
-            pl.semaphore_signal(
-                semaphore, inc=1, device_id=(at.seq + at.sides, at.group), device_id_type=MESH
-            )
+
+    def signal(semaphore, plane, side, rank, core):
+        pl.semaphore_signal(
+            semaphore,
+            inc=1,
+            device_id=(plane * at.sides + side, rank * at.cores + core),
+            device_id_type=MESH,
+        )
+
+    def signal_sides(semaphore, cores):
+        for step in range(1, at.sides):
+            for core in cores:
+                signal(semaphore, at.plane, lax.rem(at.side + step, at.sides), at.rank, core)
+
+    def signal_inner(semaphore):
+        signal(semaphore, at.inner, at.side, at.rank, at.core)
+
+    def signal_outer(semaphore):
+        @pl.when(at.has_outer)
+        def _():
+            signal(semaphore, at.outer, at.side, at.rank, at.core)
+
+    def greet():
+        if at.planes > 1:
+
+            @pl.when(at.is_middle)
+            def _():
+                for core in range(at.cores):
+                    signal(barrier, at.inner, at.side, at.rank, core)
+
+            @pl.when(at.has_outer)
+            def _():
+                for core in range(at.cores):
+                    signal(barrier, at.outer, at.side, at.rank, core)
+
+        cores = range(at.cores)
+        signal_sides(barrier, cores)
+        for step in range(1, at.ranks):
+            for core in cores:
+                signal(barrier, at.plane, at.side, lax.rem(at.rank + step, at.ranks), core)
+        for step in range(1, at.cores):
+            signal(barrier, at.plane, at.side, at.rank, lax.rem(at.core + step, at.cores))
+
+    def meet():
+        columns_met = at.sides + at.ranks - 1 + (at.planes > 1)
+        pl.semaphore_wait(barrier, columns_met * at.cores - 1)
+        signal_sides(round_sem.at[0], (at.core,))
+
+    def pass_inwards():
+        @pl.when(at.is_middle)
+        def _():
+            signal_inner(round_sem.at[2])
+
+        @pl.when(jnp.logical_not(at.is_middle))
+        def _():
+            signal_inner(round_sem.at[1])
+
+    def meet_plane():
+        pl.semaphore_wait(round_sem.at[0], at.sides - 1)
+        if at.planes > 1:
+            pl.when(jnp.logical_not(at.has_outer))(pass_inwards)
+
+    def meet_outer():
+        if at.planes > 1:
+
+            @pl.when(at.has_outer)
+            def _():
+                pl.semaphore_wait(round_sem.at[1], 1)
+                pass_inwards()
+
+    def meet_planes():
+        if at.planes > 1:
+
+            @pl.when(at.is_middle)
+            def _():
+                pl.semaphore_wait(round_sem.at[2], 1)
+
+            @pl.when(jnp.logical_not(at.is_middle))
+            def _():
+                pl.semaphore_wait(round_sem.at[3], 1)
+
+            signal_outer(round_sem.at[3])
 
     near = at.near_half()
     x_copy(near).start()
     small_copies[0].start()
     w_copy(0, 0).start()
     w_copy(0, 1).start()
-    signal_column(barrier)
-
-    @pl.loop(0, at.per_plane)
-    def _(peer):
-        device = at.plane * at.per_plane + peer
-
-        @pl.when(device != me)
-        def _():
-            pl.semaphore_signal(
-                barrier,
-                inc=1,
-                device_id=(device // groups, lax.rem(device, groups)),
-                device_id_type=MESH,
-            )
-
+    greet()
     x_copy(near).wait()
     small_copies[0].wait()
     for turn in range(1, groups):
@@ -210,18 +271,6 @@
         @pl.when(half != near)
         def _():
             x_copy(half).start()
-
-    rounds = at.planes - 1
-    if rounds == 0:
-        pl.semaphore_wait(barrier, at.per_plane - 1)
-    else:
-        pl.semaphore_wait(barrier, at.per_plane - 1 + below + above)
-        signal_column(round_sem.at[0])
-
-    def finish_round(number):
-        pl.semaphore_wait(round_sem.at[number], below + above)
-        if number + 1 < rounds:
-            signal_column(round_sem.at[number + 1])
 
     def block_rows(device):
         return pl.ds(pl.multiple_of(device * positions, positions), positions)
@@ -234,8 +283,8 @@
         return device, pltpu.make_async_remote_copy(
             src_ref=outgoing.at[half, turn, :, cols],
             dst_ref=arrived.at[block_rows(me), cols],
-            send_sem=send_sem.at[device],
-            recv_sem=recv_sem.at[me],
+            send_sem=send_sem,
+            recv_sem=recv_sem.at[at.plane * at.sides + lax.rem(half, at.sides)],
             device_id=(seq, group),
             device_id_type=MESH,
         )
@@ -251,6 +300,11 @@
         def _():
             cols = slice(part * columns, (part + 1) * columns)
             arrived[block_rows(me), cols] = outgoing[half, turn, :, cols]
+
+    def launch_both(index):
+        half, turn = at.place(index)
+        launch(half, turn, 0)
+        launch(half, turn, 1)
 
     def norm(half):
         @pl.loop(0, positions // NORM_ROWS)
@@ -274,6 +328,8 @@
             normed[...], weight[turn], preferred_element_type=jnp.float32
         ).astype(jnp.bfloat16)
 
+    stages = (meet_plane, meet_outer, meet_planes)
+
     @pl.loop(0, devices)
     def _(index):
         half, turn = at.place(index)
@@ -294,23 +350,40 @@
 
         project(half, turn, 0)
 
-        @pl.when(index > 0)
-        def _():
-            last_half, last_turn = at.place(index - 1)
-            launch(last_half, last_turn, 1)
+        @pl.when(index == 0)
+        def _():
+            meet()
+
+        @pl.when((index > 0) & (index <= EARLY))
+        def _():
+            early_half, early_turn = at.place(index - 1)
+            launch(early_half, early_turn, 1)
 
         @pl.when(fresh)
         def _():
             w_copy(turn, 1).wait()
 
         project(half, turn, 1)
-        for number in range(rounds):
-
-            @pl.when(index == min(number, EARLY))
+
+        for number, stage in enumerate(stages):
+
+            @pl.when(index == 2 + number)
             def _():
-                finish_round(number)
-
-        launch(half, turn, 0)
+                stage()
+
+        @pl.when(index < EARLY)
+        def _():
+            launch(half, turn, 0)
+
+        @pl.when(index == EARLY + LAG)
+        def _():
+            @pl.loop(EARLY, EARLY + LAG)
+            def _(number):
+                launch_both(number)
+
+        @pl.when(index > EARLY + LAG)
+        def _():
+            launch_both(index - 1)
 
     small_copies[1].wait()
     small_copies[2].wait()
@@ -328,50 +401,52 @@
             score_row == head, offset[at.group * local_heads + head], head_offsets
         )
     offsets[...] = head_offsets
-    last_half, last_turn = at.place(jnp.int32(devices - 1))
-    launch(last_half, last_turn, 1)
+    launch_both(jnp.int32(devices - 1))
 
     earlier = later_matrix(positions)
 
-    def wait_block(source):
-        @pl.when(source != me)
-        def _():
-            pltpu.make_async_copy(
-                outgoing.at[0, 0], arrived.at[block_rows(source)], recv_sem.at[source]
-            ).wait()
-
-    @pl.loop(0, devices // BATCH - 1)
-    def _(batch):
-        sources = [at.source(batch * BATCH + k) for k in range(BATCH)]
-        for source in sources:
-            wait_block(source)
-        for source in sources:
-            rows = block_rows(source)
-            reading, rest = read_block(
-                masked_query[...],
-                offsets[...],
-                earlier,
-                arrived[rows, :columns],
-                arrived[rows, columns:],
-                head_dim,
-            )
-            block_read[source] = reading
-            block_rest[source] = rest
-
-    @pl.loop(0, devices)
-    def _(index):
-        half = index // groups
-        turn = lax.rem(index, groups)
-        device = at.send_seq(half) * groups + at.send_group(turn)
-
-        @pl.when(device != me)
-        def _():
-            pltpu.make_async_copy(
-                outgoing.at[half, turn], arrived.at[block_rows(device)], send_sem.at[device]
-            ).wait()
-
-    for k in range(BATCH):
-        wait_block(at.source(jnp.int32(devices - BATCH + k)))
+    def wait_group(number):
+        plane = at.source_plane(number // at.sides)
+        half = lax.rem(number, at.sides)
+        semaphore = recv_sem.at[plane * at.sides + half]
+
+        def wait_blocks(count):
+            whole = arrived.at[pl.ds(0, count * positions)]
+            pltpu.make_async_copy(whole, whole, semaphore).wait()
+
+        with_own = (plane == at.plane) & (half == at.straight())
+
+        @pl.when(with_own)
+        def _():
+            wait_blocks(groups - 1)
+
+        @pl.when(jnp.logical_not(with_own))
+        def _():
+            wait_blocks(groups)
+
+    @pl.loop(0, seqs - 1)
+    def _(number):
+        wait_group(number)
+
+        @pl.loop(0, groups // BATCH)
+        def _(batch):
+            for k in range(BATCH):
+                source = at.source(number * groups + batch * BATCH + k)
+                rows = block_rows(source)
+                reading, rest = read_block(
+                    masked_query[...],
+                    offsets[...],
+                    earlier,
+                    arrived[rows, :columns],
+                    arrived[rows, columns:],
+                    head_dim,
+                )
+                block_read[source] = reading
+                block_rest[source] = rest
+
+    sent = arrived.at[pl.ds(0, (devices - 1) * positions)]
+    pltpu.make_async_copy(sent, sent, send_sem).wait()
+    wait_group(jnp.int32(seqs - 1))
 
 
 def finish_kernel(
@@ -402,7 +477,7 @@
     span = length // pieces
 
     def out_copies(piece):
-        rows = pl.ds(piece * span, span)
+        rows = pl.ds(pl.multiple_of(piece * span, span), span)
         return (
             pltpu.make_async_copy(
                 arrived.at[rows, pl.ds(0, columns)], keys_hbm.at[rows], out_sem.at[0, piece]
@@ -412,11 +487,12 @@
             ),
         )
 
-    for piece in range(pieces):
+    @pl.loop(0, pieces)
+    def _(piece):
         for copy in out_copies(piece):
             copy.start()
 
-    sources = [at.source(jnp.int32(devices - BATCH + k)) for k in range(BATCH)]
+    sources = [at.source(jnp.int32(devices - groups + k)) for k in range(groups)]
     earlier = later_matrix(positions)
     last_read[...] = block_read[...]
     last_rest[...] = block_rest[...]
@@ -447,9 +523,11 @@
         )
     read_copy = pltpu.make_async_copy(read, read_hbm, read_sem)
     read_copy.start(priority=1)
-    for piece in range(pieces):
+    @pl.loop(0, pieces)
+    def _(piece):
         for copy in out_copies(piece):
             copy.wait()
+
     read_copy.wait()
 
 
@@ -486,9 +564,9 @@
             pltpu.SemaphoreType.DMA((seq_count,)),
             pltpu.SemaphoreType.DMA((2, groups)),
             pltpu.SemaphoreType.DMA((3,)),
-            pltpu.SemaphoreType.DMA((devices,)),
-            pltpu.SemaphoreType.DMA((devices,)),
-            pltpu.SemaphoreType.REGULAR((seqs,)),
+            pltpu.SemaphoreType.DMA,
+            pltpu.SemaphoreType.DMA((seqs,)),
+            pltpu.SemaphoreType.REGULAR((4,)),
         ],
         compiler_params=pltpu.CompilerParams(
             collective_id=0, has_side_effects=True, vmem_limit_bytes=VMEM_BYTES - passed_bytes

time: 102 us -> 100 us (0.980)
  Pallas kernels: 100 us -> 98.4 us
where the time goes in v3:
time: 100 us; the launch traced here: 99 us
  Pallas kernels  98.4 us (98%)
    pallas_call x1, Pallas kernels, shards(): pl.pallas_call(functools.partial(exchange_kernel, seqs, groups, local_hea...  96.3 us
    pallas_call x1, Pallas kernels, shards(): pl.pallas_call(functools.partial(finish_kernel, seqs, groups, local_heads...  2.1 us

profile of v3, /device:TPU:13, one launch (start us, length us, event | category | flops | bytes accessed | tf_op | source)
XLA Modules:
  0.0 99.0 jit_solution(4907585639648450189)
XLA Ops:
  0.6 96.3 %shard_map.85 = (bf16[4096,512]{1,0:T(8,128)(2,1)S(1)}, f32[32,8,256]{2,1,0:T(8,128)S(1)}, f32[32,8,128]{2,1,0:T(8,128)S(1)}, bf16[8,256]{1,0:T(8,128)(2,1)S(1)}, f32[8,128]{1,0:T(8,128)S(1)}) custom-call(bf16[8,128,2048]{2,1,0:T(8,128)(2,1)} %x_hbm.1, bf16[2048]{0:T(1024)(128)(2,1)} %gain_hbm.1, bf16[2048,1024]{1,0:T(8,128)(2,1)} %key_w_hbm.1, ...), custom_call_target="tpu_custom_call" | custom-call | tf_op jit(solution)/shard_map/pallas_call | solution.py:544
  96.9 2.1 %shard_map.86 = (bf16[4096,256]{1,0:T(8,128)(2,1)}, bf16[4096,256]{1,0:T(8,128)(2,1)}, f32[1,256]{1,0:T(1,128)}) custom-call(bf16[4096,512]{1,0:T(8,128)(2,1)S(1)} %get-tuple-element.11.arrived, f32[32,8,256]{2,1,0:T(8,128)S(1)} %get-tuple-element.12.block_read, f32[32,8,128]{2,1,0:T(8,128)S(1)} %get-tuple-element.13.block_rest, ...), custom_call_target="tpu_custom_call" | custom-call | tf_op jit(solution)/shard_map/pallas_call | solution.py:575

commit v4 on v3

--- a/solution.py
+++ b/solution.py
@@ -57,12 +57,24 @@
     def straight(self):
         return lax.rem(self.sides - self.core, self.sides)
 
+    def opens(self, index):
+        first = self.near_half() * self.groups
+        late = index - EARLY
+        late = late + EARLY * (late >= first).astype(jnp.int32)
+        return (index >= EARLY) & (lax.rem(late, self.groups) == 0)
+
     def place(self, index):
         first = self.near_half() * self.groups
         late = index - EARLY
         late = late + EARLY * (late >= first).astype(jnp.int32)
         number = jnp.where(index < EARLY, first + index, late)
-        return number // self.groups, lax.rem(number, self.groups)
+        half = number // self.groups
+        turn = lax.rem(number, self.groups)
+        if self.planes > 2:
+            last_half = self.near_half() - self.straight() + self.sides - 1
+            turned = lax.rem(turn + self.cores * (self.ranks - self.rank), self.groups)
+            turn = jnp.where((half == last_half) & (self.core == 0), turned, turn)
+        return half, turn
 
     def send_group(self, turn):
         rank = lax.rem(self.rank + turn // self.cores, self.ranks)
@@ -255,9 +267,9 @@
     near = at.near_half()
     x_copy(near).start()
     small_copies[0].start()
+    greet()
     w_copy(0, 0).start()
     w_copy(0, 1).start()
-    greet()
     x_copy(near).wait()
     small_copies[0].wait()
     for turn in range(1, groups):
@@ -333,12 +345,13 @@
     @pl.loop(0, devices)
     def _(index):
         half, turn = at.place(index)
-
-        @pl.when((turn == 0) & (half != near))
+        opens = at.opens(index)
+
+        @pl.when(opens & (half != near))
         def _():
             x_copy(half).wait()
 
-        @pl.when((turn == 0) | (index == EARLY) | ((half == near) & (turn == EARLY)))
+        @pl.when(opens | (index == 0) | (index == EARLY) | ((half == near) & (turn == EARLY)))
         def _():
             norm(half)
 
@@ -353,6 +366,7 @@
         @pl.when(index == 0)
         def _():
             meet()
+            launch(half, turn, 0)
 
         @pl.when((index > 0) & (index <= EARLY))
         def _():
@@ -371,7 +385,7 @@
             def _():
                 stage()
 
-        @pl.when(index < EARLY)
+        @pl.when((index > 0) & (index < EARLY))
         def _():
             launch(half, turn, 0)
 

time: 100 us -> 98.3 us (0.983)
  no operation moved by 1% of the time
where the time goes in v4:
time: 98.3 us; the launch traced here: 98.2 us
  Pallas kernels  97.5 us (99%)
    pallas_call x1, Pallas kernels, shards(): pl.pallas_call(functools.partial(exchange_kernel, seqs, groups, local_hea...  95.4 us
    pallas_call x1, Pallas kernels, shards(): pl.pallas_call(functools.partial(finish_kernel, seqs, groups, local_heads...  2.1 us

profile of v4, /device:TPU:13, one launch (start us, length us, event | category | flops | bytes accessed | tf_op | source)
XLA Modules:
  0.0 98.2 jit_solution(14597362916956137876)
XLA Ops:
  0.6 95.4 %shard_map.85 = (bf16[4096,512]{1,0:T(8,128)(2,1)S(1)}, f32[32,8,256]{2,1,0:T(8,128)S(1)}, f32[32,8,128]{2,1,0:T(8,128)S(1)}, bf16[8,256]{1,0:T(8,128)(2,1)S(1)}, f32[8,128]{1,0:T(8,128)S(1)}) custom-call(bf16[8,128,2048]{2,1,0:T(8,128)(2,1)} %x_hbm.1, bf16[2048]{0:T(1024)(128)(2,1)} %gain_hbm.1, bf16[2048,1024]{1,0:T(8,128)(2,1)} %key_w_hbm.1, ...), custom_call_target="tpu_custom_call" | custom-call | tf_op jit(solution)/shard_map/pallas_call | solution.py:558
  96.1 2.1 %shard_map.86 = (bf16[4096,256]{1,0:T(8,128)(2,1)}, bf16[4096,256]{1,0:T(8,128)(2,1)}, f32[1,256]{1,0:T(1,128)}) custom-call(bf16[4096,512]{1,0:T(8,128)(2,1)S(1)} %get-tuple-element.11.arrived, f32[32,8,256]{2,1,0:T(8,128)S(1)} %get-tuple-element.12.block_read, f32[32,8,128]{2,1,0:T(8,128)S(1)} %get-tuple-element.13.block_rest, ...), custom_call_target="tpu_custom_call" | custom-call | tf_op jit(solution)/shard_map/pallas_call | solution.py:589

commit v5 on v4

--- a/solution.py
+++ b/solution.py
@@ -72,7 +72,8 @@
         turn = lax.rem(number, self.groups)
         if self.planes > 2:
             last_half = self.near_half() - self.straight() + self.sides - 1
-            turned = lax.rem(turn + self.cores * (self.ranks - self.rank), self.groups)
+            shift = jnp.where(self.side == 0, self.ranks - self.rank, 1)
+            turned = lax.rem(turn + self.cores * shift, self.groups)
             turn = jnp.where((half == last_half) & (self.core == 0), turned, turn)
         return half, turn
 

time: 98.3 us -> 98.3 us (level)
  no operation moved by 1% of the time
where the time goes in v5:
time: 98.3 us; the launch traced here: 98.2 us
  Pallas kernels  97.5 us (99%)
    pallas_call x1, Pallas kernels, shards(): pl.pallas_call(functools.partial(exchange_kernel, seqs, groups, local_hea...  95.4 us
    pallas_call x1, Pallas kernels, shards(): pl.pallas_call(functools.partial(finish_kernel, seqs, groups, local_heads...  2.1 us

profile of v5, /device:TPU:13, one launch (start us, length us, event | category | flops | bytes accessed | tf_op | source)
XLA Modules:
  0.0 98.2 jit_solution(1997040910590614380)
XLA Ops:
  0.6 95.4 %shard_map.85 = (bf16[4096,512]{1,0:T(8,128)(2,1)S(1)}, f32[32,8,256]{2,1,0:T(8,128)S(1)}, f32[32,8,128]{2,1,0:T(8,128)S(1)}, bf16[8,256]{1,0:T(8,128)(2,1)S(1)}, f32[8,128]{1,0:T(8,128)S(1)}) custom-call(bf16[8,128,2048]{2,1,0:T(8,128)(2,1)} %x_hbm.1, bf16[2048]{0:T(1024)(128)(2,1)} %gain_hbm.1, bf16[2048,1024]{1,0:T(8,128)(2,1)} %key_w_hbm.1, ...), custom_call_target="tpu_custom_call" | custom-call | tf_op jit(solution)/shard_map/pallas_call | solution.py:559
  96.1 2.1 %shard_map.86 = (bf16[4096,256]{1,0:T(8,128)(2,1)}, bf16[4096,256]{1,0:T(8,128)(2,1)}, f32[1,256]{1,0:T(1,128)}) custom-call(bf16[4096,512]{1,0:T(8,128)(2,1)S(1)} %get-tuple-element.11.arrived, f32[32,8,256]{2,1,0:T(8,128)S(1)} %get-tuple-element.12.block_read, f32[32,8,128]{2,1,0:T(8,128)S(1)} %get-tuple-element.13.block_rest, ...), custom_call_target="tpu_custom_call" | custom-call | tf_op jit(solution)/shard_map/pallas_call | solution.py:590
